TPU v7x, 32 devices: a whole 2x2x4 slice. The times are simulated.
32 devices in a mesh: ep: 32 (over z, y, x, core).
Axes of the slice: x: 2, y: 2, z: 4, core: 2. Of those that a mesh axis runs over, the one named last changes fastest.
Arguments:
- tokens: bfloat16 [128, 2048], P('ep'), may hold values from -6 to 6
- recurrent_state: float32 [128, 8, 128, 128], P('ep'), may hold values from -4 to 4
- query_weight: bfloat16 [2048, 1024], P(None, 'ep'), may hold values from -0.125 to 0.125
- forget_weight: bfloat16 [2048, 1024], P(None, 'ep'), may hold values from -0.125 to 0.125
- input_weight: bfloat16 [2048, 1024], P(None, 'ep'), may hold values from -0.125 to 0.125
- outgate_weight: bfloat16 [2048, 1024], P(None, 'ep'), may hold values from -0.125 to 0.125
- lower_bound: float32 [1024], replicated, may hold values from 0 to 0.9
- head_gain: float32 [128], replicated, may hold values from 0.1 to 1.9
- mixout_weight: bfloat16 [1024, 2048], P(None, 'ep'), may hold values from -0.1875 to 0.1875
- first_gain: float32 [2048], replicated, may hold values from 0.1 to 1.9
- first_bias: float32 [2048], replicated, may hold values from -1.5 to 1.5
- router_weight: bfloat16 [2048, 8], replicated, may hold values from -0.125 to 0.125
- branch_vector: bfloat16 [2048], replicated, may hold values from -0.125 to 0.125
- dense_gate_weight: bfloat16 [2048, 5632], P(None, 'ep'), may hold values from -0.125 to 0.125
- dense_up_weight: bfloat16 [2048, 5632], P(None, 'ep'), may hold values from -0.125 to 0.125
- dense_down_weight: bfloat16 [5632, 2048], P('ep'), may hold values from -0.078125 to 0.078125
- expert_gate_weight: bfloat16 [2048, 57344], P(None, 'ep'), may hold values from -0.125 to 0.125
- expert_up_weight: bfloat16 [2048, 57344], P(None, 'ep'), may hold values from -0.125 to 0.125
- expert_down_weight: bfloat16 [57344, 2048], P('ep'), may hold values from -0.0625 to 0.0625
- second_gain: float32 [2048], replicated, may hold values from 0.1 to 1.9
- second_bias: float32 [2048], replicated, may hold values from -1.5 to 1.5
- routes: int32 [128, 2], replicated, may hold values from 0 to 7, all different within a row; in each aligned block of 4 rows (0 to 3, 4 to 7, ...) at most 2 rows name the same one
Outputs:
- output: bfloat16 [128, 2048], P('ep')
- new_state: float32 [128, 8, 128, 128], P('ep')
Inputs may be any that keep to these rules, and one draw needn't show every extreme that they name: `routes`: each row names two different experts; in the rows of one device no expert is named more than 2 times, a bound that some block reaches in some device's rows.
All inputs are finite; a program needn't handle non-finite values.
Results may differ from a plain program's by a relative error of at most 0.0095.
Values may be sent and summed in bfloat16 or wider, within the bound.
No kernel may reach another device: no remote copies, remote signals or barrier semaphores. Data moves between devices by JAX's collectives and lax.ppermute only.
A program may use at most 64 MiB of HBM per device.

v0:
```python
import jax
import jax.numpy as jnp
from jax import lax
from jax.sharding import PartitionSpec as P

EXPERTS = 8
CAP = 2


ALPHA = 8.0**0.25
NORM_EPS = 1e-05
HEAD_EPS = 1e-06


def layer_norm(mixture, gain, bias):
    center = jnp.mean(mixture, axis=-1, keepdims=True)
    spread = jnp.mean(jnp.square(mixture - center), axis=-1, keepdims=True)
    return (mixture - center) * lax.rsqrt(spread + NORM_EPS) * gain + bias


def recurrence(projected, state, lower_bound, head_gain):
    nseq, heads, width = (state.shape[0], state.shape[1], state.shape[2])
    query = projected[:, 0].astype(jnp.float32).reshape(nseq, heads, width)
    forget_in = projected[:, 1].astype(jnp.float32)
    value = projected[:, 2].astype(jnp.float32).reshape(nseq, heads, width)
    outgate = projected[:, 3].astype(jnp.float32)
    forget = (lower_bound + (1.0 - lower_bound) * jax.nn.sigmoid(forget_in)).reshape(
        nseq, heads, width
    )
    keyed = ((1.0 - lower_bound) * jax.nn.sigmoid(-forget_in)).reshape(nseq, heads, width)
    fresh = forget[..., None] * state + keyed[..., None] * value[:, :, None, :]
    read = jnp.einsum("bhkv,bhk->bhv", fresh, query, precision=lax.Precision.HIGHEST)
    scaled = (
        read * lax.rsqrt(jnp.mean(jnp.square(read), axis=-1, keepdims=True) + HEAD_EPS) * head_gain
    )
    mixed = (scaled.reshape(nseq, heads * width) * jax.nn.silu(outgate)).astype(jnp.bfloat16)
    return (mixed, fresh)


def route_share(rows, picks, router_weight):
    f32 = jnp.float32
    logits = jnp.dot(rows, router_weight, preferred_element_type=f32)
    expert_ids = jnp.arange(EXPERTS, dtype=jnp.int32)
    first_logit = jnp.sum(jnp.where(picks[:, 0:1] == expert_ids[None, :], logits, 0.0), axis=1)
    second_logit = jnp.sum(jnp.where(picks[:, 1:2] == expert_ids[None, :], logits, 0.0), axis=1)
    return jax.nn.sigmoid(first_logit - second_logit)


def channel_term(
    with_experts,
    normed_all,
    routes,
    start,
    count,
    router_weight,
    branch_vector,
    dense_gate_weight,
    dense_up_weight,
    dense_down_weight,
    expert_gate_weight,
    expert_up_weight,
    expert_down_weight,
):
    f32 = jnp.float32
    branch_gate = jax.nn.sigmoid(jnp.dot(normed_all, branch_vector, preferred_element_type=f32))
    dense_hidden = (
        jax.nn.silu(jnp.dot(normed_all, dense_gate_weight, preferred_element_type=f32))
        * jnp.dot(normed_all, dense_up_weight, preferred_element_type=f32)
    ).astype(jnp.bfloat16)
    dense_part = branch_gate[:, None] * jnp.dot(
        dense_hidden, dense_down_weight, preferred_element_type=f32
    )
    return dense_part


def expert_slots(
    own_rows, own_picks, router_weight, expert_gate_weight, expert_up_weight, expert_down_weight
):
    f32 = jnp.float32
    width = own_rows.shape[1]
    share = route_share(own_rows, own_picks, router_weight)
    expert_ids = jnp.arange(EXPERTS, dtype=jnp.int32)
    on_first = own_picks[None, :, 0] == expert_ids[:, None]
    on_second = own_picks[None, :, 1] == expert_ids[:, None]
    token_weight = share[None, :] * on_first.astype(f32) + (1.0 - share)[
        None, :
    ] * on_second.astype(f32)
    hits = (on_first | on_second).astype(jnp.int32)
    ranks = jnp.cumsum(hits, axis=1) - 1
    slot_ids = jnp.arange(CAP, dtype=jnp.int32)
    select = (ranks[:, None, :] == slot_ids[None, :, None]) & (hits[:, None, :] > 0)
    slot_rows = jnp.einsum(
        "eci,id->ecd", select.astype(jnp.bfloat16), own_rows, preferred_element_type=f32
    ).astype(jnp.bfloat16)
    spread_count = lax.axis_size("ep") // EXPERTS
    sent = jnp.repeat(slot_rows, spread_count, axis=0)
    arrived = lax.all_to_all(sent, "ep", split_axis=0, concat_axis=0, tiled=True)
    flat = arrived.reshape(-1, width)
    gate_part = jnp.dot(flat, expert_gate_weight, preferred_element_type=f32)
    up_part = jnp.dot(flat, expert_up_weight, preferred_element_type=f32)
    hidden = (jax.nn.silu(gate_part) * up_part).astype(jnp.bfloat16)
    made = jnp.dot(hidden, expert_down_weight, preferred_element_type=f32).reshape(arrived.shape)
    returned = lax.all_to_all(
        made.astype(jnp.bfloat16), "ep", split_axis=0, concat_axis=0, tiled=True
    ).astype(made.dtype)
    summed = jnp.sum(returned.reshape(EXPERTS, spread_count, CAP, width), axis=1)
    back = jnp.einsum("eci,ecd->eid", select.astype(f32), summed, precision=lax.Precision.HIGHEST)
    return jnp.sum(back * token_weight[:, :, None], axis=0)


def per_device(
    tokens,
    recurrent_state,
    query_weight,
    forget_weight,
    input_weight,
    outgate_weight,
    lower_bound,
    head_gain,
    mixout_weight,
    first_gain,
    first_bias,
    router_weight,
    branch_vector,
    dense_gate_weight,
    dense_up_weight,
    dense_down_weight,
    expert_gate_weight,
    expert_up_weight,
    expert_down_weight,
    second_gain,
    second_bias,
    routes,
):
    f32 = jnp.float32
    devices = lax.axis_size("ep")
    nseq, width = tokens.shape
    own_cols = query_weight.shape[1]
    row_start = lax.axis_index("ep") * nseq
    own_picks = lax.dynamic_slice_in_dim(routes, row_start, nseq, 0)
    stacked = jnp.concatenate([query_weight, forget_weight, input_weight, outgate_weight], axis=1)
    weights = (
        router_weight,
        branch_vector,
        dense_gate_weight,
        dense_up_weight,
        dense_down_weight,
        expert_gate_weight,
        expert_up_weight,
        expert_down_weight,
    )
    gathered = jnp.dot(
        lax.all_gather(tokens, "ep", axis=0, tiled=True), stacked, preferred_element_type=f32
    ).astype(jnp.bfloat16)
    owned = lax.all_to_all(gathered, "ep", split_axis=0, concat_axis=1, tiled=True)
    projected = (
        owned.reshape(nseq, devices, 4, own_cols)
        .transpose(0, 2, 1, 3)
        .reshape(nseq, 4, devices * own_cols)
    )
    mixed, new_state = recurrence(projected, recurrent_state, lower_bound, head_gain)
    mix_cols = jnp.dot(
        lax.all_gather(mixed, "ep", axis=0, tiled=True), mixout_weight, preferred_element_type=f32
    ).astype(jnp.bfloat16)
    mix_out = lax.all_to_all(mix_cols, "ep", split_axis=0, concat_axis=1, tiled=True)
    normed = layer_norm(
        ALPHA * tokens.astype(f32) + mix_out.astype(f32), first_gain, first_bias
    ).astype(jnp.bfloat16)
    normed_all = lax.all_gather(normed, "ep", axis=0, tiled=True)
    channel = lax.psum_scatter(
        channel_term(False, normed_all, routes, jnp.int32(0), nseq * lax.axis_size("ep"), *weights),
        "ep",
        scatter_dimension=0,
        tiled=True,
    )
    channel = channel + expert_slots(
        normed, own_picks, router_weight, expert_gate_weight, expert_up_weight, expert_down_weight
    )
    output = layer_norm(ALPHA * normed.astype(f32) + channel, second_gain, second_bias).astype(
        jnp.bfloat16
    )
    return (output, new_state)


def solution(mesh):
    return jax.shard_map(
        per_device,
        mesh=mesh,
        in_specs=(
            P("ep", None),
            P("ep", None, None, None),
            P(None, "ep"),
            P(None, "ep"),
            P(None, "ep"),
            P(None, "ep"),
            P(),
            P(),
            P(None, "ep"),
            P(),
            P(),
            P(),
            P(),
            P(None, "ep"),
            P(None, "ep"),
            P("ep", None),
            P(None, "ep"),
            P(None, "ep"),
            P("ep", None),
            P(),
            P(),
            P(),
        ),
        out_specs=(P("ep", None), P("ep", None, None, None)),
        check_vma=False,
    )
```

profile of v0, /device:TPU:0, one launch (start us, length us, event | category | flops | bytes accessed | tf_op | source)
XLA Modules:
  0.0 312.9 jit_solution(12458948402277351714)
XLA Ops:
  7.2 0.0 copy-start
  7.2 0.0 copy-start.2
  7.2 0.0 copy-start.10
  7.2 0.0 copy-start.3
  7.2 0.0 copy-start.9
  7.2 0.0 copy-start.6
  7.2 45.1 %all-gather = bf16[32,4,2048]{2,1,0:T(4,128)(2,1)S(1)} all-gather(bf16[1,4,2048]{2,1,0:T(4,128)(2,1)} %bitcast.89), channel_id=1, replica_groups=mesh['ep'=32] {'ep'}, dimensions={0}, use_global_device_ids=true | all-gather | bytes 540672 | tf_op jit(solution)/shard_map/all_gather | solution.py:153
  52.3 0.1 reshape.316
  52.4 2.0 convolution_convert_fusion.2
  54.4 2.6 all-to-all-start
  57.0 0.7 subtract_bitcast_fusion
  57.7 0.7 constant_dynamic-slice_fusion
  58.5 0.5 copy-done.7
  59.0 0.2 reduce_window_sum.11
  59.1 5.1 %all-to-all-done = bf16[32,4,128]{2,1,0:T(4,128)(2,1)S(1)} async-done(((bf16[32,4,128]{2,1,0:T(4,128)(2,1)}), bf16[32,4,128]{2,1,0:T(4,128)(2,1)S(1)}, u32[]{:S(2)}, u32[]{:S(2)}) %all-to-all-start) | async-done | bytes 32800 | tf_op jit(solution)/shard_map/all_to_all | solution.py:155
  64.3 0.1 reshape.300
  64.4 0.2 reshape.301
  64.6 0.1 add_divide_fusion.1
  64.7 0.7 multiply_add_fusion.2
  65.4 2.5 multiply_add_fusion
  67.9 0.0 copy-start.1
  67.9 1.1 fusion.28
  69.0 0.1 multiply_reduce_fusion.2
  69.1 0.1 multiply_bitcast_fusion
  69.2 37.6 %all-gather.1 = bf16[32,4,1024]{2,1,0:T(4,128)(2,1)S(1)} all-gather(bf16[1,4,1024]{2,1,0:T(4,128)(2,1)S(1)} %fusion.34), channel_id=1, replica_groups=mesh['ep'=32] {'ep'}, dimensions={0}, use_global_device_ids=true | all-gather | bytes 270336 | tf_op jit(solution)/shard_map/all_gather | solution.py:163
  106.8 0.1 reshape.318
  106.8 0.0 copy-done.3
  106.8 0.2 convolution_convert_fusion.3
  107.1 0.1 copy.44
  107.2 0.7 reshape.327
  107.9 2.5 all-to-all-start.1
  110.5 7.0 %all-to-all-done.1 = bf16[32,2,128]{2,1,0:T(2,128)(2,1)S(1)} async-done(((bf16[32,2,128]{2,1,0:T(2,128)(2,1)}), bf16[32,2,128]{2,1,0:T(2,128)(2,1)S(1)}, u32[]{:S(2)}, u32[]{:S(2)}) %all-to-all-start.1) | async-done | bytes 16416 | tf_op jit(solution)/shard_map/all_to_all | solution.py:165
  117.5 0.1 reshape.328
  117.7 0.1 reshape.312
  117.7 0.0 copy-done.2
  117.7 0.1 fusion.37
  117.9 0.2 multiply_reduce_fusion.1
  118.1 0.1 add_convert_fusion.1
  118.2 40.9 %all-gather.2 = bf16[32,4,2048]{2,1,0:T(4,128)(2,1)} all-gather(bf16[1,4,2048]{2,1,0:T(4,128)(2,1)S(1)} %bitcast.90), channel_id=1, replica_groups=mesh['ep'=32] {'ep'}, dimensions={0}, use_global_device_ids=true | all-gather | bytes 540672 | tf_op jit(solution)/shard_map/all_gather | solution.py:169
  159.1 1.2 reshape.320
  160.3 0.1 convolution_convert_fusion.1
  160.4 0.1 copy.47
  160.5 0.9 broadcast_in_dim.6
  161.4 3.3 %all-to-all-start.2 = ((bf16[32,2,2048]{2,1,0:T(2,128)(2,1)}), bf16[32,2,2048]{2,1,0:T(2,128)(2,1)}, u32[]{:S(2)}, u32[]{:S(2)}) async-start(bf16[32,2,2048]{2,1,0:T(2,128)(2,1)} %bitcast.87), calls=%async_computation.2 | async-start | bytes 524288 | tf_op jit(solution)/shard_map/all_to_all | solution.py:97
  164.7 0.0 all-reduce.3.cloned.1.call-start
  164.7 1.5 fusion.43
  166.2 0.2 fusion.6
  166.4 3.1 convolution_multiply_fusion
  169.5 0.0 all-reduce.3.cloned.1.call-update
  169.6 5.7 %all-to-all-done.2 = bf16[32,2,2048]{2,1,0:T(2,128)(2,1)} async-done(((bf16[32,2,2048]{2,1,0:T(2,128)(2,1)}), bf16[32,2,2048]{2,1,0:T(2,128)(2,1)}, u32[]{:S(2)}, u32[]{:S(2)}) %all-to-all-start.2) | async-done | bytes 262176 | tf_op jit(solution)/shard_map/all_to_all | solution.py:97
  175.2 1.0 reshape.305
  176.3 4.6 %fusion.44 = f32[64,1792]{1,0:T(8,128)S(1)} fusion(bf16[64,2048]{1,0:T(8,128)(2,1)S(1)} %reshape.305, bf16[2048,1792]{1,0:T(8,128)(2,1)} %param.38), kind=kOutput, calls=%fused_computation.94 | convolution fusion | flops 469762048 | bytes 8060928 | tf_op jit(solution)/shard_map/dot_general | solution.py:99
  180.9 8.7 %convolution_convert_fusion = bf16[64,2048]{1,0:T(8,128)(2,1)} fusion(bf16[1792,2048]{1,0:T(8,128)(2,1)} %param.40, bf16[64,2048]{1,0:T(8,128)(2,1)S(1)} %reshape.305, bf16[2048,1792]{1,0:T(8,128)(2,1)} %param.39, f32[64,1792]{1,0:T(8,128)S(1)} %fusion.44), kind=kOutput, calls=%fused_computation.3 | convolution fusion | flops 940343296 | bytes 15663104 | tf_op jit(solution)/shard_map/dot_general | solution.py:102
  189.5 1.9 convert_element_type.112
  191.4 2.6 all-to-all-start.3
  194.0 1.0 select_reduce_fusion
  195.1 0.7 select_add_fusion
  195.7 9.5 %all-to-all-done.3 = bf16[32,2,2048]{2,1,0:T(2,128)(2,1)S(1)} async-done(((bf16[32,2,2048]{2,1,0:T(2,128)(2,1)}), bf16[32,2,2048]{2,1,0:T(2,128)(2,1)S(1)}, u32[]{:S(2)}, u32[]{:S(2)}) %all-to-all-start.3) | async-done | bytes 262176 | tf_op jit(solution)/shard_map/all_to_all | solution.py:103
  205.2 0.2 convert_reduce_fusion
  205.5 1.1 fusion.1
  206.6 96.8 %all-reduce.3.cloned.1.call-done = f32[128,2048]{1,0:T(8,128)} async-done(((f32[128,2048]{1,0:T(8,128)}), f32[128,2048]{1,0:T(8,128)}) %all-reduce.3.cloned.1.call-update) | async-done | bytes 1048592
  303.5 1.0 fusion.41
  304.5 0.2 multiply_reduce_fusion
  304.7 1.4 add_convert_fusion
  (29 shorter events, 0.2 us)
Async XLA Ops:
  7.2 159.3 %copy-start = (bf16[176,2048]{1,0:T(8,128)(2,1)S(1)}, bf16[176,2048]{1,0:T(8,128)(2,1)}, u32[]{:S(2)}) copy-start(bf16[176,2048]{1,0:T(8,128)(2,1)} %param.37) | copy-start | bytes 2162692
  7.2 110.6 %copy-start.2 = (bf16[4,2048]{1,0:T(4,128)(2,1)S(1)}, bf16[4,2048]{1,0:T(4,128)(2,1)}, u32[]{:S(2)}) copy-start(bf16[4,2048]{1,0:T(4,128)(2,1)} %param.22) | copy-start | bytes 49156
  7.2 61.9 %copy-start.10 = (f32[128]{0:T(128)S(1)}, f32[128]{0:T(128)}, u32[]{:S(2)}) copy-start(f32[128]{0:T(128)} %param.29) | copy-start | bytes 1540
  7.2 99.6 %copy-start.3 = (bf16[1024,64]{0,1:T(8,128)(2,1)S(1)}, bf16[1024,64]{0,1:T(8,128)(2,1)}, u32[]{:S(2)}) copy-start(bf16[1024,64]{0,1:T(8,128)(2,1)} %param.30) | copy-start | bytes 393220
  7.2 103.3 %copy-start.9 = (bf16[2048]{0:T(1024)(128)(2,1)S(1)}, bf16[2048]{0:T(1024)(128)(2,1)}, u32[]{:S(2)}) copy-start(bf16[2048]{0:T(1024)(128)(2,1)} %param.34) | copy-start | bytes 12292
  7.2 110.9 %copy-start.6 = (f32[2048]{0:T(1024)S(1)}, f32[2048]{0:T(1024)}, u32[]{:S(2)}) copy-start(f32[2048]{0:T(1024)} %param.31) | copy-start | bytes 24580
  7.2 110.9 %copy-start.5 = (f32[2048]{0:T(1024)S(1)}, f32[2048]{0:T(1024)}, u32[]{:S(2)}) copy-start(f32[2048]{0:T(1024)} %param.32) | copy-start | bytes 24580
  54.4 9.8 %all-to-all-start = ((bf16[32,4,128]{2,1,0:T(4,128)(2,1)}), bf16[32,4,128]{2,1,0:T(4,128)(2,1)S(1)}, u32[]{:S(2)}, u32[]{:S(2)}) async-start(bf16[32,4,128]{2,1,0:T(4,128)(2,1)} %bitcast.4), calls=%async_computation | async-start | bytes 65536 | tf_op jit(solution)/shard_map/all_to_all | solution.py:155
  58.5 0.5 copy-start.7
  58.5 52.0 %copy-start.8 = (s32[4]{0:T(128)}, s32[4]{0:T(128)S(1)}, u32[]{:S(2)}) copy-start(s32[4]{0:T(128)S(1)} %get-tuple-element.17) | copy-start | bytes 52
  67.9 113.0 %copy-start.1 = (f32[4,8,128,128]{3,2,1,0:T(8,128)}, f32[4,8,128,128]{3,2,1,0:T(8,128)S(1)}, u32[]{:S(2)}) copy-start(f32[4,8,128,128]{3,2,1,0:T(8,128)S(1)} %multiply_add_fusion) | copy-start | bytes 6291460
  107.9 9.7 %all-to-all-start.1 = ((bf16[32,2,128]{2,1,0:T(2,128)(2,1)}), bf16[32,2,128]{2,1,0:T(2,128)(2,1)S(1)}, u32[]{:S(2)}, u32[]{:S(2)}) async-start(bf16[32,2,128]{2,1,0:T(2,128)(2,1)} %reshape.327), calls=%async_computation.1 | async-start | bytes 32768 | tf_op jit(solution)/shard_map/all_to_all | solution.py:165
  110.5 64.8 %copy-start.4 = (pred[8,2,4]{2,1,0:T(4,128)(4,1)}, pred[8,2,4]{2,1,0:T(4,128)(4,1)S(1)}, u32[]{:S(2)}) copy-start(pred[8,2,4]{2,1,0:T(4,128)(4,1)S(1)} %compare_and_fusion) | copy-start | bytes 196
  161.4 13.9 %all-to-all-start.2 = ((bf16[32,2,2048]{2,1,0:T(2,128)(2,1)}), bf16[32,2,2048]{2,1,0:T(2,128)(2,1)}, u32[]{:S(2)}, u32[]{:S(2)}) async-start(bf16[32,2,2048]{2,1,0:T(2,128)(2,1)} %bitcast.87), calls=%async_computation.2 | async-start | bytes 524288 | tf_op jit(solution)/shard_map/all_to_all | solution.py:97
  164.7 138.8 %all-reduce.3.cloned.1.call-start = ((), (), s32[]{:S(2)}) async-start(), calls=%async_computation.4 | async-start | bytes 2097152
  191.4 13.8 %all-to-all-start.3 = ((bf16[32,2,2048]{2,1,0:T(2,128)(2,1)}), bf16[32,2,2048]{2,1,0:T(2,128)(2,1)S(1)}, u32[]{:S(2)}, u32[]{:S(2)}) async-start(bf16[32,2,2048]{2,1,0:T(2,128)(2,1)} %convert_element_type.112), calls=%async_computation.3 | async-start | bytes 524288 | tf_op jit(solution)/shard_map/all_to_all | solution.py:103
Sparse Core Ops, SparseCore 0:
  170.7 132.7 all-reduce.2
where the time goes:
time: 314 us; the launch traced here: 313 us
  blocking collectives  124 us (39%)
  waiting for transfers between devices  124 us (39%)
  matrix products  23.6 us (8%)
  between operations  14.4 us (5%)
  starting transfers between devices  11 us (4%)
  other arithmetic  8.33 us (3%)
  local copies, waits for them, and re-layouts  7.81 us (2%)
    unnamed x2, waiting for transfers between devices  96.9 us
    all_gather x1, blocking collectives, per_device(): lax.all_gather(tokens, 'ep', axis=0, tiled=True)  45.1 us
    all_gather x1, blocking collectives, per_device(): normed_all = lax.all_gather(normed, 'ep', axis=0, tiled=True)  40.9 us
    all_gather x1, blocking collectives, per_device(): lax.all_gather(mixed, 'ep', axis=0, tiled=True)  37.6 us
    all_to_all x1, waiting for transfers between devices, expert_slots(): lax.all_to_all(made.astype(jnp.bfloat16), 'ep', split_axis=0, concat_axis...  9.5 us
    dot_general x1, matrix products, expert_slots(): jnp.dot(hidden, expert_down_weight, preferred_element_type=f32)  8.66 us
    all_to_all x1, waiting for transfers between devices, per_device(): lax.all_to_all(mix_cols, 'ep', split_axis=0, concat_axis=1, tiled=True)  7.02 us
  transfers between devices with their start and end apart: 5, of which 5 were waited for; matrix products, arithmetic and copies ran while one was open for 8% of the time, Pallas kernels for 0%

commit v1 on v0

v1 whole, which is shorter than its diff:
```python
import jax
import jax.numpy as jnp
from jax import lax
from jax.sharding import PartitionSpec as P

ALPHA = 8.0**0.25
NORM_EPS = 1e-05
HEAD_EPS = 1e-06


def layer_norm(mixture, gain, bias):
    center = jnp.mean(mixture, axis=-1, keepdims=True)
    spread = jnp.mean(jnp.square(mixture - center), axis=-1, keepdims=True)
    return (mixture - center) * lax.rsqrt(spread + NORM_EPS) * gain + bias


def recurrence(projected, state, lower_bound, head_gain):
    nseq, heads, width = (state.shape[0], state.shape[1], state.shape[2])
    query = projected[:, 0].astype(jnp.float32).reshape(nseq, heads, width)
    forget_in = projected[:, 1].astype(jnp.float32)
    value = projected[:, 2].astype(jnp.float32).reshape(nseq, heads, width)
    outgate = projected[:, 3].astype(jnp.float32)
    forget = (lower_bound + (1.0 - lower_bound) * jax.nn.sigmoid(forget_in)).reshape(
        nseq, heads, width
    )
    keyed = ((1.0 - lower_bound) * jax.nn.sigmoid(-forget_in)).reshape(nseq, heads, width)
    fresh = forget[..., None] * state + keyed[..., None] * value[:, :, None, :]
    read = jnp.einsum("bhkv,bhk->bhv", fresh, query, precision=lax.Precision.HIGHEST)
    scaled = (
        read * lax.rsqrt(jnp.mean(jnp.square(read), axis=-1, keepdims=True) + HEAD_EPS) * head_gain
    )
    mixed = (scaled.reshape(nseq, heads * width) * jax.nn.silu(outgate)).astype(jnp.bfloat16)
    return (mixed, fresh)


def gather_all(block):
    devices = lax.axis_size("ep")
    copies = jnp.broadcast_to(block[None], (devices,) + block.shape)
    return lax.all_to_all(copies, "ep", split_axis=0, concat_axis=0, tiled=True)


def expert_weight(logits, routes, expert):
    expert_ids = jnp.arange(logits.shape[1], dtype=jnp.int32)
    first_logit = jnp.sum(jnp.where(routes[:, 0:1] == expert_ids[None, :], logits, 0.0), axis=1)
    second_logit = jnp.sum(jnp.where(routes[:, 1:2] == expert_ids[None, :], logits, 0.0), axis=1)
    share = jax.nn.sigmoid(first_logit - second_logit)
    return jnp.where(
        routes[:, 0] == expert, share, jnp.where(routes[:, 1] == expert, 1.0 - share, 0.0)
    )


def gated_hidden(rows, gate_weight, up_weight):
    f32 = jnp.float32
    return (
        jax.nn.silu(jnp.dot(rows, gate_weight, preferred_element_type=f32))
        * jnp.dot(rows, up_weight, preferred_element_type=f32)
    ).astype(jnp.bfloat16)


def per_device(
    tokens,
    recurrent_state,
    query_weight,
    forget_weight,
    input_weight,
    outgate_weight,
    lower_bound,
    head_gain,
    mixout_weight,
    first_gain,
    first_bias,
    router_weight,
    branch_vector,
    dense_gate_weight,
    dense_up_weight,
    dense_down_weight,
    expert_gate_weight,
    expert_up_weight,
    expert_down_weight,
    second_gain,
    second_bias,
    routes,
):
    f32 = jnp.float32
    bf16 = jnp.bfloat16
    devices = lax.axis_size("ep")
    nseq, width = tokens.shape
    own_cols = query_weight.shape[1]
    experts = router_weight.shape[1]
    own_index = lax.axis_index("ep")
    row_start = own_index * nseq
    own_expert = own_index // (devices // experts)

    stacked = jnp.concatenate([query_weight, forget_weight, input_weight, outgate_weight], axis=1)
    tokens_all = gather_all(tokens).reshape(devices * nseq, width)
    gathered = jnp.dot(tokens_all, stacked, preferred_element_type=f32).astype(bf16)
    owned = lax.all_to_all(gathered, "ep", split_axis=0, concat_axis=1, tiled=True)
    projected = (
        owned.reshape(nseq, devices, 4, own_cols)
        .transpose(0, 2, 1, 3)
        .reshape(nseq, 4, devices * own_cols)
    )
    mixed, new_state = recurrence(projected, recurrent_state, lower_bound, head_gain)

    mixed_all = gather_all(mixed).reshape(devices * nseq, -1)
    mix_rows = lax.dot_general(
        mixout_weight, mixed_all, (((0,), (1,)), ((), ())), preferred_element_type=f32
    ).astype(bf16)
    mix_out = gather_all(mix_rows).reshape(width, devices * nseq).T
    normed_all = layer_norm(
        ALPHA * tokens_all.astype(f32) + mix_out.astype(f32), first_gain, first_bias
    ).astype(bf16)
    own_normed = lax.dynamic_slice_in_dim(normed_all, row_start, nseq, 0)

    logits = jnp.dot(normed_all, router_weight, preferred_element_type=f32)
    weight = expert_weight(logits, routes, own_expert)
    branch_gate = jax.nn.sigmoid(jnp.dot(normed_all, branch_vector, preferred_element_type=f32))
    dense_hidden = gated_hidden(normed_all, dense_gate_weight, dense_up_weight)
    hidden = gated_hidden(normed_all, expert_gate_weight, expert_up_weight)
    partial = branch_gate[:, None] * jnp.dot(
        dense_hidden, dense_down_weight, preferred_element_type=f32
    ) + weight[:, None] * jnp.dot(hidden, expert_down_weight, preferred_element_type=f32)
    returned = lax.all_to_all(
        partial.astype(bf16).reshape(devices, nseq, width),
        "ep",
        split_axis=0,
        concat_axis=0,
        tiled=True,
    )
    channel = jnp.sum(returned.astype(f32), axis=0)
    output = layer_norm(ALPHA * own_normed.astype(f32) + channel, second_gain, second_bias).astype(
        bf16
    )
    return (output, new_state)


def solution(mesh):
    return jax.shard_map(
        per_device,
        mesh=mesh,
        in_specs=(
            P("ep", None),
            P("ep", None, None, None),
            P(None, "ep"),
            P(None, "ep"),
            P(None, "ep"),
            P(None, "ep"),
            P(),
            P(),
            P(None, "ep"),
            P(),
            P(),
            P(),
            P(),
            P(None, "ep"),
            P(None, "ep"),
            P("ep", None),
            P(None, "ep"),
            P(None, "ep"),
            P("ep", None),
            P(),
            P(),
            P(),
        ),
        out_specs=(P("ep", None), P("ep", None, None, None)),
        check_vma=False,
    )
```

time: 314 us -> 118 us (0.38)
  blocking collectives: 124 us -> 35.1 us
  waiting for transfers between devices: 124 us -> 37.7 us
  between operations: 14.4 us -> 0.98 us
  matrix products: 23.6 us -> 20.3 us
    all_gather x3 -> x0, blocking collectives: 124 us -> none  [the longest x1 45.1 us: per_device(): lax.all_gather(tokens, 'ep', axis=0, tiled=True)]
    unnamed x2 -> x0, waiting for transfers between devices: 96.9 us -> none
    all_to_all x0 -> x2, blocking collectives: none -> 35.1 us  [gather_all(): return lax.all_to_all(copies, 'ep', split_axis=0, concat_axis=0, tiled=True)]
    all_to_all x3 -> x2, waiting for transfers between devices: 22.2 us -> 31.1 us  [the longest x1 15.6 us: per_device(): lax.all_to_all(partial.astype(bf16).reshape(devices, nseq, width), 'ep',...]
    dot_general x10 -> x8, matrix products: 22.6 us -> 19.3 us  [the longest x1 8.01 us: per_device(): jnp.dot(hidden, expert_down_weight, preferred_element_type=f32)]
    all_to_all x3 -> x2, starting transfers between devices: 8.43 us -> 5.49 us  [the longest x1 2.89 us: per_device(): lax.all_to_all(partial.astype(bf16).reshape(devices, nseq, width), 'ep',...]
  transfers between devices with their start and end apart: 5 -> 3, of which waited for: 5 -> 3; matrix products, arithmetic and copies ran while one was open for 8% -> 1% of each run, Pallas kernels for 0% -> 0%
where the time goes in v1:
time: 118 us
  waiting for transfers between devices  37.7 us (32%)
  blocking collectives  35.1 us (30%)
  matrix products  20.3 us (17%)
  local copies, waits for them, and re-layouts  9.14 us (8%)
  starting transfers between devices  8.46 us (7%)
  other arithmetic  6.15 us (5%)
    all_to_all x2, blocking collectives, gather_all(): return lax.all_to_all(copies, 'ep', split_axis=0, concat_axis=0, tiled=True)  35.1 us
    all_to_all x1, waiting for transfers between devices, per_device(): lax.all_to_all(partial.astype(bf16).reshape(devices, nseq, width), 'ep',...  15.6 us
    all_to_all x1, waiting for transfers between devices, gather_all(): return lax.all_to_all(copies, 'ep', split_axis=0, concat_axis=0, tiled=True)  15.5 us
    dot_general x1, matrix products, per_device(): jnp.dot(hidden, expert_down_weight, preferred_element_type=f32)  8.01 us
    all_to_all x1, waiting for transfers between devices, per_device(): lax.all_to_all(gathered, 'ep', split_axis=0, concat_axis=1, tiled=True)  6.56 us
    dot_general x2, matrix products, gated_hidden(): jnp.dot(rows, gate_weight, preferred_element_type=f32)  6.21 us
    all_to_all x1, starting transfers between devices, per_device(): lax.all_to_all(gathered, 'ep', split_axis=0, concat_axis=1, tiled=True)  2.97 us
    all_to_all x1, starting transfers between devices, per_device(): lax.all_to_all(partial.astype(bf16).reshape(devices, nseq, width), 'ep',...  2.89 us
  transfers between devices with their start and end apart: 3, of which 3 were waited for; matrix products, arithmetic and copies ran while one was open for 1% of the time, Pallas kernels for 0%

profile of v1, /device:TPU:0, one launch (start us, length us, event | category | flops | bytes accessed | tf_op | source)
XLA Modules:
  0.0 117.9 jit_solution(11621133900110692437)
XLA Ops:
  0.6 0.0 copy-start
  0.6 0.0 copy-start.2
  0.7 0.0 copy-start.13
  0.7 1.1 broadcast_in_dim.13
  1.8 22.9 %all_to_all.36 = bf16[32,4,2048]{2,1,0:T(4,128)(2,1)} all-to-all(bf16[32,4,2048]{2,1,0:T(4,128)(2,1)S(1)} %broadcast_in_dim.13), channel_id=1, replica_groups=mesh['ep'=32] {'ep'}, dimensions={0} | all-to-all | bytes 1048576 | tf_op jit(solution)/shard_map/all_to_all | solution.py:39
  24.6 1.2 %reshape.185 = bf16[128,2048]{1,0:T(8,128)(2,1)S(1)} reshape(bf16[32,4,2048]{2,1,0:T(4,128)(2,1)} %all_to_all.36) | data formatting | bytes 1048576 | tf_op jit(solution)/shard_map/reshape | solution.py:95
  25.8 2.0 %convolution_convert_fusion = bf16[128,128]{0,1:T(8,128)(2,1)} fusion(bf16[128,2048]{1,0:T(8,128)(2,1)S(1)} %reshape.185, bf16[2048,32]{0,1:T(8,128)(2,1)} %param.27, bf16[2048,32]{0,1:T(8,128)(2,1)} %param.26, bf16[2048,32]{0,1:T(8,128)(2,1)} %param.25, bf16[2048,32]{0,1:T(8,128)(2,1)} %param.24), kind=kOutput, calls=%fused_computation.9 | convolution fusion | flops 69222400 | bytes 1081344 | tf_op jit(solution)/shard_map/dot_general | solution.py:96
  27.8 3.0 %all-to-all-start.1 = ((bf16[32,4,128]{2,1,0:T(4,128)(2,1)}), bf16[32,4,128]{2,1,0:T(4,128)(2,1)S(1)}, u32[]{:S(2)}, u32[]{:S(2)}) async-start(bf16[32,4,128]{2,1,0:T(4,128)(2,1)} %bitcast.3), calls=%async_computation.1 | async-start | bytes 65536 | tf_op jit(solution)/shard_map/all_to_all | solution.py:97
  30.8 0.7 subtract_bitcast_fusion
  31.5 6.6 %all-to-all-done.1 = bf16[32,4,128]{2,1,0:T(4,128)(2,1)S(1)} async-done(((bf16[32,4,128]{2,1,0:T(4,128)(2,1)}), bf16[32,4,128]{2,1,0:T(4,128)(2,1)S(1)}, u32[]{:S(2)}, u32[]{:S(2)}) %all-to-all-start.1) | async-done | bytes 32800 | tf_op jit(solution)/shard_map/all_to_all | solution.py:97
  38.1 0.1 reshape.186
  38.2 0.7 copy.31
  38.9 1.1 reshape.187
  40.0 0.1 add_divide_fusion.1
  40.1 0.7 multiply_add_fusion.2
  40.8 0.0 copy-done.2
  40.8 0.0 copy-start.8
  40.8 1.3 %multiply_add_fusion = f32[4,8,128,128]{3,2,1,0:T(8,128)S(1)} fusion(f32[4,8,128,128]{3,2,1,0:T(8,128)S(1)} %copy-done.2, f32[4,8,128]{2,1,0:T(8,128)S(1)} %bitcast.91, f32[4,8,128]{2,1,0:T(8,128)S(1)} %get-tuple-element.11, f32[4,8,128]{2,1,0:T(8,128)S(1)} %get-tuple-element.10), kind=kLoop, calls=%fused_computation.6 | loop fusion | flops 1572864 | bytes 4243456 | tf_op jit(solution)/shard_map/add | solution.py:27
  42.1 0.0 copy-start.1
  42.1 1.3 %copy-done.1 = f32[4,8,128,128]{3,2,1,0:T(8,128)} copy-done((f32[4,8,128,128]{3,2,1,0:T(8,128)}, f32[4,8,128,128]{3,2,1,0:T(8,128)S(1)}, u32[]{:S(2)}) %copy-start.1) | copy-done | bytes 2097176
  43.4 1.1 fusion.25
  44.5 0.1 multiply_reduce_fusion.2
  44.6 0.0 copy-done.13
  44.6 0.1 multiply_bitcast_fusion
  44.7 0.1 broadcast_in_dim.14
  44.8 12.3 %all_to_all.37 = bf16[32,4,1024]{2,1,0:T(4,128)(2,1)S(1)} all-to-all(bf16[32,4,1024]{2,1,0:T(4,128)(2,1)S(1)} %broadcast_in_dim.14), channel_id=1, replica_groups=mesh['ep'=32] {'ep'}, dimensions={0} | all-to-all | bytes 524288 | tf_op jit(solution)/shard_map/all_to_all | solution.py:39
  57.1 0.1 reshape.190
  57.1 0.0 copy-done.5
  57.1 0.2 fusion.4
  57.3 0.9 broadcast_in_dim.15
  58.2 2.6 %all-to-all-start.3 = ((bf16[32,64,128]{2,1,0:T(8,128)(2,1)}), bf16[32,64,128]{2,1,0:T(8,128)(2,1)S(1)}, u32[]{:S(2)}, u32[]{:S(2)}) async-start(bf16[32,64,128]{2,1,0:T(8,128)(2,1)} %broadcast_in_dim.15), calls=%async_computation.3 | async-start | bytes 1048576 | tf_op jit(solution)/shard_map/all_to_all | solution.py:39
  60.9 0.0 copy-done.11
  60.9 0.0 copy-done.12
  60.9 15.5 %all-to-all-done.3 = bf16[32,64,128]{2,1,0:T(8,128)(2,1)S(1)} async-done(((bf16[32,64,128]{2,1,0:T(8,128)(2,1)}), bf16[32,64,128]{2,1,0:T(8,128)(2,1)S(1)}, u32[]{:S(2)}, u32[]{:S(2)}) %all-to-all-start.3) | async-done | bytes 524320 | tf_op jit(solution)/shard_map/all_to_all | solution.py:39
  76.5 1.1 bitcast_convert_fusion
  77.5 1.6 %copy.32 = f32[2048,128]{0,1:T(8,128)S(1)} copy(f32[2048,128]{1,0:T(8,128)} %bitcast_convert_fusion) | data formatting | bytes 2097152 | tf_op jit(solution)/shard_map/convert_element_type | solution.py:111
  79.1 0.2 fusion.17
  79.3 0.3 multiply_reduce_fusion
  79.7 0.0 copy-done.7
  79.7 0.0 copy-done.8
  79.7 0.3 add_convert_fusion
  80.0 0.0 copy-start.3
  80.0 0.0 copy-start.6
  80.0 5.2 %fusion.35 = f32[128,1792]{1,0:T(8,128)} fusion(bf16[128,2048]{1,0:T(8,128)(2,1)S(1)} %add_convert_fusion, bf16[2048,1792]{1,0:T(8,128)(2,1)} %param.38), kind=kOutput, calls=%fused_computation.78 | convolution fusion | flops 939524096 | bytes 8781824 | tf_op jit(solution)/shard_map/dot_general | solution.py:55
  85.2 0.0 copy-done.3
  85.2 1.0 fusion.34
  86.2 0.8 fusion.8
  87.0 0.0 copy-done.6
  87.0 0.2 select_reduce_fusion
  87.3 0.0 copy-start.4
  87.3 0.0 copy-start.9
  87.3 0.0 copy-start.10
  87.3 8.0 %convolution_multiply_fusion.1 = f32[128,2048]{1,0:T(8,128)S(1)} fusion(bf16[1792,2048]{1,0:T(8,128)(2,1)} %param.40, bf16[128,2048]{1,0:T(8,128)(2,1)S(1)} %add_convert_fusion, bf16[2048,1792]{1,0:T(8,128)(2,1)} %param.39, f32[128,1792]{1,0:T(8,128)} %fusion.35, f32[128]{0:T(128)S(1)} %fusion.29), kind=kOutput, calls=%fused_computation.1 | convolution fusion | flops 1880686592 | bytes 17170944 | tf_op jit(solution)/shard_map/dot_general | solution.py:122
  95.3 0.0 copy-done
  95.3 0.0 copy-done.4
  95.3 1.8 %fusion.2 = bf16[128,2048]{1,0:T(8,128)(2,1)S(1)} fusion(f32[128,2048]{1,0:T(8,128)S(1)} %convolution_multiply_fusion.1, bf16[176,2048]{1,0:T(8,128)(2,1)S(1)} %copy-done, bf16[128,2048]{1,0:T(8,128)(2,1)S(1)} %add_convert_fusion, bf16[2048,176]{0,1:T(8,128)(2,1)S(1)} %copy-done.4, f32[128]{0:T(128)} %fusion.8, f32[128,176]{0,1:T(8,128)} %fusion.34), kind=kOutput, calls=%fused_computation.5 | convolution fusion | flops 185470976 | bytes 3629568 | tf_op jit(solution)/shard_map/dot_general | solution.py:120
  97.1 1.0 reshape.191
  98.1 2.9 %all-to-all-start.4 = ((bf16[32,4,2048]{2,1,0:T(4,128)(2,1)}), bf16[32,4,2048]{2,1,0:T(4,128)(2,1)S(1)}, u32[]{:S(2)}, u32[]{:S(2)}) async-start(bf16[32,4,2048]{2,1,0:T(4,128)(2,1)} %reshape.191), calls=%async_computation.4 | async-start | bytes 1048576 | tf_op jit(solution)/shard_map/all_to_all | solution.py:123
  101.0 15.6 %all-to-all-done.4 = bf16[32,4,2048]{2,1,0:T(4,128)(2,1)S(1)} async-done(((bf16[32,4,2048]{2,1,0:T(4,128)(2,1)}), bf16[32,4,2048]{2,1,0:T(4,128)(2,1)S(1)}, u32[]{:S(2)}, u32[]{:S(2)}) %all-to-all-start.4) | async-done | bytes 524320 | tf_op jit(solution)/shard_map/all_to_all | solution.py:123
  116.6 0.2 convert_reduce_fusion
  116.9 0.1 fusion.33
  117.0 0.2 multiply_reduce_fusion.1
  117.2 0.0 copy-done.9
  117.2 0.7 add_convert_fusion.1
  (16 shorter events, 0.1 us)
Async XLA Ops:
  0.6 94.7 %copy-start = (bf16[176,2048]{1,0:T(8,128)(2,1)S(1)}, bf16[176,2048]{1,0:T(8,128)(2,1)}, u32[]{:S(2)}) copy-start(bf16[176,2048]{1,0:T(8,128)(2,1)} %param.37) | copy-start | bytes 2162692
  0.6 40.2 %copy-start.2 = (f32[4,8,128,128]{3,2,1,0:T(8,128)S(1)}, f32[4,8,128,128]{3,2,1,0:T(8,128)}, u32[]{:S(2)}) copy-start(f32[4,8,128,128]{3,2,1,0:T(8,128)} %param.23) | copy-start | bytes 6291460
  0.7 43.9 %copy-start.13 = (f32[128]{0:T(128)S(1)}, f32[128]{0:T(128)}, u32[]{:S(2)}) copy-start(f32[128]{0:T(128)} %param.29) | copy-start | bytes 1540
  24.6 36.2 %copy-start.11 = (bf16[2048]{0:T(1024)(128)(2,1)S(1)}, bf16[2048]{0:T(1024)(128)(2,1)}, u32[]{:S(2)}) copy-start(bf16[2048]{0:T(1024)(128)(2,1)} %param.34) | copy-start | bytes 12292
  24.6 36.3 %copy-start.12 = (s32[128,2]{0,1:T(2,128)S(1)}, s32[128,2]{0,1:T(2,128)}, u32[]{:S(2)}) copy-start(s32[128,2]{0,1:T(2,128)} %param.43) | copy-start | bytes 3076
  27.8 10.2 %all-to-all-start.1 = ((bf16[32,4,128]{2,1,0:T(4,128)(2,1)}), bf16[32,4,128]{2,1,0:T(4,128)(2,1)S(1)}, u32[]{:S(2)}, u32[]{:S(2)}) async-start(bf16[32,4,128]{2,1,0:T(4,128)(2,1)} %bitcast.3), calls=%async_computation.1 | async-start | bytes 65536 | tf_op jit(solution)/shard_map/all_to_all | solution.py:97
  38.9 18.2 %copy-start.5 = (bf16[1024,64]{0,1:T(8,128)(2,1)S(1)}, bf16[1024,64]{0,1:T(8,128)(2,1)}, u32[]{:S(2)}) copy-start(bf16[1024,64]{0,1:T(8,128)(2,1)} %param.30) | copy-start | bytes 393220
  40.8 38.8 %copy-start.7 = (f32[2048]{0:T(1024)S(1)}, f32[2048]{0:T(1024)}, u32[]{:S(2)}) copy-start(f32[2048]{0:T(1024)} %param.32) | copy-start | bytes 24580
  40.8 38.8 %copy-start.8 = (f32[2048]{0:T(1024)S(1)}, f32[2048]{0:T(1024)}, u32[]{:S(2)}) copy-start(f32[2048]{0:T(1024)} %param.31) | copy-start | bytes 24580
  42.1 1.3 %copy-start.1 = (f32[4,8,128,128]{3,2,1,0:T(8,128)}, f32[4,8,128,128]{3,2,1,0:T(8,128)S(1)}, u32[]{:S(2)}) copy-start(f32[4,8,128,128]{3,2,1,0:T(8,128)S(1)} %multiply_add_fusion) | copy-start | bytes 6291460
  58.2 18.2 %all-to-all-start.3 = ((bf16[32,64,128]{2,1,0:T(8,128)(2,1)}), bf16[32,64,128]{2,1,0:T(8,128)(2,1)S(1)}, u32[]{:S(2)}, u32[]{:S(2)}) async-start(bf16[32,64,128]{2,1,0:T(8,128)(2,1)} %broadcast_in_dim.15), calls=%async_computation.3 | async-start | bytes 1048576 | tf_op jit(solution)/shard_map/all_to_all | solution.py:39
  80.0 5.2 %copy-start.3 = (bf16[2048,176]{0,1:T(8,128)(2,1)S(1)}, bf16[2048,176]{0,1:T(8,128)(2,1)}, u32[]{:S(2)}) copy-start(bf16[2048,176]{0,1:T(8,128)(2,1)} %param.35) | copy-start | bytes 2162692
  80.0 7.0 %copy-start.6 = (bf16[2048,8]{0,1:T(8,128)(2,1)S(1)}, bf16[2048,8]{0,1:T(8,128)(2,1)}, u32[]{:S(2)}) copy-start(bf16[2048,8]{0,1:T(8,128)(2,1)} %param.33) | copy-start | bytes 98308
  87.3 8.1 %copy-start.4 = (bf16[2048,176]{0,1:T(8,128)(2,1)S(1)}, bf16[2048,176]{0,1:T(8,128)(2,1)}, u32[]{:S(2)}) copy-start(bf16[2048,176]{0,1:T(8,128)(2,1)} %param.36) | copy-start | bytes 2162692
  87.3 29.9 %copy-start.9 = (f32[2048]{0:T(1024)S(1)}, f32[2048]{0:T(1024)}, u32[]{:S(2)}) copy-start(f32[2048]{0:T(1024)} %param.42) | copy-start | bytes 24580
  87.3 29.9 %copy-start.10 = (f32[2048]{0:T(1024)S(1)}, f32[2048]{0:T(1024)}, u32[]{:S(2)}) copy-start(f32[2048]{0:T(1024)} %param.41) | copy-start | bytes 24580
  98.1 18.5 %all-to-all-start.4 = ((bf16[32,4,2048]{2,1,0:T(4,128)(2,1)}), bf16[32,4,2048]{2,1,0:T(4,128)(2,1)S(1)}, u32[]{:S(2)}, u32[]{:S(2)}) async-start(bf16[32,4,2048]{2,1,0:T(4,128)(2,1)} %reshape.191), calls=%async_computation.4 | async-start | bytes 1048576 | tf_op jit(solution)/shard_map/all_to_all | solution.py:123

commit v2 on v1

--- a/solution.py
+++ b/solution.py
@@ -1,6 +1,8 @@
 import jax
 import jax.numpy as jnp
 from jax import lax
+from jax.experimental import pallas as pl
+from jax.experimental.pallas import tpu as pltpu
 from jax.sharding import PartitionSpec as P
 
 ALPHA = 8.0**0.25
@@ -39,22 +41,119 @@
     return lax.all_to_all(copies, "ep", split_axis=0, concat_axis=0, tiled=True)
 
 
-def expert_weight(logits, routes, expert):
-    expert_ids = jnp.arange(logits.shape[1], dtype=jnp.int32)
-    first_logit = jnp.sum(jnp.where(routes[:, 0:1] == expert_ids[None, :], logits, 0.0), axis=1)
-    second_logit = jnp.sum(jnp.where(routes[:, 1:2] == expert_ids[None, :], logits, 0.0), axis=1)
-    share = jax.nn.sigmoid(first_logit - second_logit)
-    return jnp.where(
-        routes[:, 0] == expert, share, jnp.where(routes[:, 1] == expert, 1.0 - share, 0.0)
-    )
-
-
-def gated_hidden(rows, gate_weight, up_weight):
+def hidden_block(extent):
+    for size in (256, 128):
+        if extent % size == 0:
+            return size
+    return extent
+
+
+def channel_kernel(
+    mix_ref,
+    tokens_ref,
+    gain_ref,
+    bias_ref,
+    router_ref,
+    pick_ref,
+    first_ref,
+    second_ref,
+    dense_gate_hbm,
+    dense_up_hbm,
+    dense_down_hbm,
+    gate_hbm,
+    up_hbm,
+    down_hbm,
+    partial_ref,
+    normed_ref,
+    dense_gate,
+    dense_up,
+    dense_down,
+    gate,
+    up,
+    down,
+    acc_ref,
+    sems,
+    dense_sems,
+):
     f32 = jnp.float32
-    return (
-        jax.nn.silu(jnp.dot(rows, gate_weight, preferred_element_type=f32))
-        * jnp.dot(rows, up_weight, preferred_element_type=f32)
-    ).astype(jnp.bfloat16)
+    bf16 = jnp.bfloat16
+    extent = gate_hbm.shape[1]
+    block = hidden_block(extent)
+    spans = [pl.ds(at, block) for at in range(0, extent, block)]
+    copies = []
+    for step, span in enumerate(spans):
+        copies.append(
+            (
+                pltpu.make_async_copy(gate_hbm.at[:, span], gate.at[:, span], sems.at[0, step]),
+                pltpu.make_async_copy(up_hbm.at[:, span], up.at[:, span], sems.at[1, step]),
+                pltpu.make_async_copy(down_hbm.at[span, :], down.at[span, :], sems.at[2, step]),
+            )
+        )
+    dense_copies = (
+        pltpu.make_async_copy(dense_gate_hbm, dense_gate, dense_sems.at[0]),
+        pltpu.make_async_copy(dense_up_hbm, dense_up, dense_sems.at[1]),
+        pltpu.make_async_copy(dense_down_hbm, dense_down, dense_sems.at[2]),
+    )
+    for copy in dense_copies:
+        copy.start()
+    for group in copies:
+        for copy in group:
+            copy.start()
+
+    mixture = ALPHA * tokens_ref[...].astype(f32) + mix_ref[...].astype(f32).T
+    normed_ref[...] = layer_norm(mixture, gain_ref[...], bias_ref[...]).astype(bf16)
+    last = (((1,), (1,)), ((), ()))
+    scores = lax.dot_general(normed_ref[...], router_ref[...], last, preferred_element_type=f32)
+    branch_gate = jax.nn.sigmoid(scores[:, -1:])
+    share = jax.nn.sigmoid(jnp.sum(scores * pick_ref[...], axis=1, keepdims=True))
+    weight = first_ref[...] * share + second_ref[...] * (1.0 - share)
+
+    for copy in dense_copies:
+        copy.wait()
+    rows = normed_ref[...]
+    dense_hidden = jax.nn.silu(
+        lax.dot_general(rows, dense_gate[...], last, preferred_element_type=f32)
+    ) * lax.dot_general(rows, dense_up[...], last, preferred_element_type=f32)
+    dense_part = jnp.dot(dense_hidden.astype(bf16), dense_down[...], preferred_element_type=f32)
+    acc_ref[...] = branch_gate * dense_part
+
+    for group, span in zip(copies, spans):
+        for copy in group:
+            copy.wait()
+        rows = normed_ref[...]
+        hidden = jax.nn.silu(
+            jnp.dot(rows, gate[:, span], preferred_element_type=f32)
+        ) * jnp.dot(rows, up[:, span], preferred_element_type=f32)
+        acc_ref[...] += weight * jnp.dot(
+            hidden.astype(bf16), down[span, :], preferred_element_type=f32
+        )
+    held = partial_ref.shape[1]
+    for device in range(partial_ref.shape[0]):
+        partial_ref[device] = acc_ref[device * held : (device + 1) * held, :].astype(bf16)
+
+
+def channel_stage(nseq, mix_rows, tokens_all, gain, bias, router, pick, first, second, *weights):
+    count, width = tokens_all.shape
+    bf16 = jnp.bfloat16
+    steps = weights[3].shape[1] // hidden_block(weights[3].shape[1])
+    whole = pl.BlockSpec(memory_space=pltpu.VMEM)
+    return pl.pallas_call(
+        channel_kernel,
+        out_shape=[
+            jax.ShapeDtypeStruct((count // nseq, nseq, width), bf16),
+            jax.ShapeDtypeStruct((count, width), bf16),
+        ],
+        in_specs=[whole] * 8 + [pl.BlockSpec(memory_space=pl.ANY)] * 6,
+        out_specs=[whole] * 2,
+        scratch_shapes=[pltpu.VMEM(w.shape, bf16) for w in weights]
+        + [
+            pltpu.VMEM((count, width), jnp.float32),
+            pltpu.SemaphoreType.DMA((3, steps)),
+            pltpu.SemaphoreType.DMA((3,)),
+        ],
+        compiler_params=pltpu.CompilerParams(vmem_limit_bytes=44 * 1024 * 1024),
+        name="channel",
+    )(mix_rows, tokens_all, gain, bias, router, pick, first, second, *weights)
 
 
 def per_device(
@@ -106,22 +205,35 @@
     mix_rows = lax.dot_general(
         mixout_weight, mixed_all, (((0,), (1,)), ((), ())), preferred_element_type=f32
     ).astype(bf16)
-    mix_out = gather_all(mix_rows).reshape(width, devices * nseq).T
-    normed_all = layer_norm(
-        ALPHA * tokens_all.astype(f32) + mix_out.astype(f32), first_gain, first_bias
-    ).astype(bf16)
+    mix_out = gather_all(mix_rows).reshape(width, devices * nseq)
+
+    columns = jnp.arange(2 * experts, dtype=jnp.int32)[None, :]
+    router = jnp.concatenate(
+        [router_weight.T, jnp.zeros((experts - 1, width), bf16), branch_vector[None, :]], axis=0
+    )
+    pick = (routes[:, 0:1] == columns).astype(f32) - (routes[:, 1:2] == columns).astype(f32)
+    first = (routes[:, 0:1] == own_expert).astype(f32)
+    second = (routes[:, 1:2] == own_expert).astype(f32)
+    partial, normed_all = channel_stage(
+        nseq,
+        mix_out,
+        tokens_all,
+        first_gain[None, :],
+        first_bias[None, :],
+        router,
+        pick,
+        first,
+        second,
+        dense_gate_weight.T,
+        dense_up_weight.T,
+        dense_down_weight,
+        expert_gate_weight,
+        expert_up_weight,
+        expert_down_weight,
+    )
     own_normed = lax.dynamic_slice_in_dim(normed_all, row_start, nseq, 0)
-
-    logits = jnp.dot(normed_all, router_weight, preferred_element_type=f32)
-    weight = expert_weight(logits, routes, own_expert)
-    branch_gate = jax.nn.sigmoid(jnp.dot(normed_all, branch_vector, preferred_element_type=f32))
-    dense_hidden = gated_hidden(normed_all, dense_gate_weight, dense_up_weight)
-    hidden = gated_hidden(normed_all, expert_gate_weight, expert_up_weight)
-    partial = branch_gate[:, None] * jnp.dot(
-        dense_hidden, dense_down_weight, preferred_element_type=f32
-    ) + weight[:, None] * jnp.dot(hidden, expert_down_weight, preferred_element_type=f32)
     returned = lax.all_to_all(
-        partial.astype(bf16).reshape(devices, nseq, width),
+        partial,
         "ep",
         split_axis=0,
         concat_axis=0,

time: 118 us -> 109 us (0.924)
  matrix products: 20.3 us -> 3.28 us
  Pallas kernels: 0 us -> 10.2 us
  waiting for transfers between devices: 37.7 us -> 34.5 us
  other arithmetic: 6.15 us -> 7.56 us
  local copies, waits for them, and re-layouts: 9.14 us -> 7.8 us
    dot_general x6 -> x0, matrix products: 17.1 us -> none  [the longest x1 8.01 us: per_device(): jnp.dot(hidden, expert_down_weight, preferred_element_type=f32)]
    pallas_call x0 -> x1, Pallas kernels: none -> 10.2 us  [channel_stage(): pl.pallas_call(channel_kernel, out_shape=[jax.ShapeDtypeStruct((count //...]
    all_to_all x1, waiting for transfers between devices: 15.5 us -> 11.6 us  [gather_all(): return lax.all_to_all(copies, 'ep', split_axis=0, concat_axis=0, tiled=True)]
    unnamed x29 -> x36, local copies, waits for them, and re-layouts: 1.39 us -> 4.64 us
    convert_element_type x1 -> x0, local copies, waits for them, and re-layouts: 1.55 us -> none  [per_device(): mix_out.astype(f32)]
  transfers between devices with their start and end apart: 3 -> 3, of which waited for: 3 -> 3; matrix products, arithmetic and copies ran while one was open for 1% -> 4% of each run, Pallas kernels for 0% -> 0%
where the time goes in v2:
time: 109 us; the launch traced here: 108 us
  blocking collectives  35.2 us (32%)
  waiting for transfers between devices  34.5 us (32%)
  Pallas kernels  10.2 us (9%)
  starting transfers between devices  8.46 us (8%)
  local copies, waits for them, and re-layouts  7.8 us (7%)
  other arithmetic  7.56 us (7%)
  matrix products  3.28 us (3%)
    all_to_all x2, blocking collectives, gather_all(): return lax.all_to_all(copies, 'ep', split_axis=0, concat_axis=0, tiled=True)  35.2 us
    all_to_all x1, waiting for transfers between devices, per_device(): lax.all_to_all(partial, 'ep', split_axis=0, concat_axis=0, tiled=True)  15.6 us
    all_to_all x1, waiting for transfers between devices, gather_all(): return lax.all_to_all(copies, 'ep', split_axis=0, concat_axis=0, tiled=True)  11.6 us
    pallas_call x1, Pallas kernels, channel_stage(): pl.pallas_call(channel_kernel, out_shape=[jax.ShapeDtypeStruct((count //...  10.2 us
    all_to_all x1, waiting for transfers between devices, per_device(): lax.all_to_all(gathered, 'ep', split_axis=0, concat_axis=1, tiled=True)  7.23 us
    unnamed x36, local copies, waits for them, and re-layouts  4.64 us
    all_to_all x1, starting transfers between devices, per_device(): lax.all_to_all(gathered, 'ep', split_axis=0, concat_axis=1, tiled=True)  2.98 us
    all_to_all x1, starting transfers between devices, per_device(): lax.all_to_all(partial, 'ep', split_axis=0, concat_axis=0, tiled=True)  2.88 us
  transfers between devices with their start and end apart: 3, of which 3 were waited for; matrix products, arithmetic and copies ran while one was open for 4% of the time, Pallas kernels for 0%

profile of v2, /device:TPU:0, one launch (start us, length us, event | category | flops | bytes accessed | tf_op | source)
XLA Modules:
  0.0 107.9 jit_solution(15357731478479654917)
XLA Ops:
  0.6 0.0 copy-start
  0.6 0.0 copy-start.15
  0.7 0.0 copy-start.16
  0.7 1.0 broadcast_in_dim.14
  1.7 0.0 copy-start.11
  1.7 22.7 %all_to_all.36 = bf16[32,4,2048]{2,1,0:T(4,128)(2,1)S(1)} all-to-all(bf16[32,4,2048]{2,1,0:T(4,128)(2,1)S(1)} %broadcast_in_dim.14), channel_id=1, replica_groups=mesh['ep'=32] {'ep'}, dimensions={0} | all-to-all | bytes 1048576 | tf_op jit(solution)/shard_map/all_to_all | solution.py:41
  24.4 0.0 copy-start.10
  24.4 0.1 reshape.130.tokens_ref
  24.6 0.0 copy-done.15
  24.6 0.0 copy-done.16
  24.6 2.0 %convolution_convert_fusion = bf16[128,128]{0,1:T(8,128)(2,1)} fusion(bf16[128,2048]{1,0:T(8,128)(2,1)S(1)} %reshape.130.tokens_ref, bf16[2048,32]{0,1:T(8,128)(2,1)S(1)} %copy-done.15, bf16[2048,32]{0,1:T(8,128)(2,1)S(1)} %copy-done.16, bf16[2048,32]{0,1:T(8,128)(2,1)} %param.25, bf16[2048,32]{0,1:T(8,128)(2,1)} %param.24), kind=kOutput, calls=%fused_computation.1 | convolution fusion | flops 69222400 | bytes 1081344 | tf_op jit(solution)/shard_map/dot_general | solution.py:195
  26.6 3.0 %all-to-all-start.1 = ((bf16[32,4,128]{2,1,0:T(4,128)(2,1)}), bf16[32,4,128]{2,1,0:T(4,128)(2,1)S(1)}, u32[]{:S(2)}, u32[]{:S(2)}) async-start(bf16[32,4,128]{2,1,0:T(4,128)(2,1)} %bitcast.3), calls=%async_computation.1 | async-start | bytes 65536 | tf_op jit(solution)/shard_map/all_to_all | solution.py:196
  29.6 0.0 copy-done.11
  29.6 7.2 %all-to-all-done.1 = bf16[32,4,128]{2,1,0:T(4,128)(2,1)S(1)} async-done(((bf16[32,4,128]{2,1,0:T(4,128)(2,1)}), bf16[32,4,128]{2,1,0:T(4,128)(2,1)S(1)}, u32[]{:S(2)}, u32[]{:S(2)}) %all-to-all-start.1) | async-done | bytes 32800 | tf_op jit(solution)/shard_map/all_to_all | solution.py:196
  36.8 0.1 reshape.131
  37.0 0.2 reshape.132
  37.2 0.1 add_divide_fusion.1
  37.3 0.0 copy-done.10
  37.3 1.3 %multiply_add_fusion = f32[4,8,128,128]{3,2,1,0:T(8,128)S(1)} fusion(f32[4,8,128,128]{3,2,1,0:T(8,128)S(1)} %copy-done.10, f32[4,8,128]{2,1,0:T(8,128)S(1)} %bitcast.60, f32[4,8,128]{2,1,0:T(8,128)S(1)} %get-tuple-element.11, f32[4,8,128]{2,1,0:T(8,128)S(1)} %get-tuple-element.10), kind=kLoop, calls=%fused_computation | loop fusion | flops 1572864 | bytes 4243456 | tf_op jit(solution)/shard_map/add | solution.py:29
  38.6 0.0 copy-start.9
  38.6 1.3 %copy-done.9 = f32[4,8,128,128]{3,2,1,0:T(8,128)} copy-done((f32[4,8,128,128]{3,2,1,0:T(8,128)}, f32[4,8,128,128]{3,2,1,0:T(8,128)S(1)}, u32[]{:S(2)}) %copy-start.9) | copy-done | bytes 2097176
  39.9 0.0 copy-start.14
  39.9 1.1 fusion.9
  41.0 0.0 copy-start.2
  41.0 0.0 copy-start.3
  41.0 0.0 copy-start.6
  41.0 0.0 copy-start.7
  41.0 0.1 multiply_reduce_fusion.1
  41.1 0.0 copy-done.14
  41.1 0.1 multiply_bitcast_fusion
  41.2 0.1 broadcast_in_dim.15
  41.3 12.4 %all_to_all.37 = bf16[32,4,1024]{2,1,0:T(4,128)(2,1)S(1)} all-to-all(bf16[32,4,1024]{2,1,0:T(4,128)(2,1)S(1)} %broadcast_in_dim.15), channel_id=1, replica_groups=mesh['ep'=32] {'ep'}, dimensions={0} | all-to-all | bytes 524288 | tf_op jit(solution)/shard_map/all_to_all | solution.py:41
  53.7 0.1 reshape.135
  53.8 0.0 copy-done
  53.8 0.2 fusion
  54.0 0.9 broadcast_in_dim.16
  54.9 2.6 %all-to-all-start.3 = ((bf16[32,64,128]{2,1,0:T(8,128)(2,1)}), bf16[32,64,128]{2,1,0:T(8,128)(2,1)S(1)}, u32[]{:S(2)}, u32[]{:S(2)}) async-start(bf16[32,64,128]{2,1,0:T(8,128)(2,1)} %broadcast_in_dim.16), calls=%async_computation.3 | async-start | bytes 1048576 | tf_op jit(solution)/shard_map/all_to_all | solution.py:41
  57.5 0.0 copy-done.13
  57.6 0.0 copy-done.12
  57.6 0.6 broadcast_in_dim.20
  58.2 0.1 copy.47
  58.3 0.7 copy.46
  59.0 0.1 pad.1.clone
  59.1 0.1 convert_subtract_fusion.pick_ref
  59.2 1.5 %compare_convert_fusion = (f32[128,1]{1,0:T(8,128)S(1)}, f32[128,1]{1,0:T(8,128)}) fusion(s32[128,1]{1,0:T(8,128)S(1)} %copy.47, s32[]{:T(128)S(6)} %select_n.8, s32[128,1]{1,0:T(8,128)} %copy.46), kind=kLoop, calls=%fused_computation.16 | loop fusion | flops 512 | bytes 2052 | tf_op jit(solution)/shard_map/convert_element_type | solution.py:216
  60.7 0.9 pad_maximum_fusion.router_ref
  61.5 11.6 %all-to-all-done.3 = bf16[32,64,128]{2,1,0:T(8,128)(2,1)S(1)} async-done(((bf16[32,64,128]{2,1,0:T(8,128)(2,1)}), bf16[32,64,128]{2,1,0:T(8,128)(2,1)S(1)}, u32[]{:S(2)}, u32[]{:S(2)}) %all-to-all-start.3) | async-done | bytes 524320 | tf_op jit(solution)/shard_map/all_to_all | solution.py:41
  73.1 0.0 copy-done.1
  73.1 0.0 copy-done.2
  73.2 0.0 copy-done.3
  73.2 0.0 copy-done.6
  73.2 0.0 copy-done.7
  73.2 0.0 copy-start.5
  73.2 0.8 copy-done.5
  74.0 10.2 %channel.1 = (bf16[32,4,2048]{2,1,0:T(4,128)(2,1)S(1)}, bf16[128,2048]{1,0:T(8,128)(2,1)S(1)}) custom-call(bf16[2048,128]{1,0:T(8,128)(2,1)S(1)} %bitcast.51, bf16[128,2048]{1,0:T(8,128)(2,1)S(1)} %reshape.130.tokens_ref, f32[1,2048]{1,0:T(1,128)S(1)} %bitcast.54, f32[1,2048]{1,0:T(1,128)S(1)} %bitcast.55, bf16[16,2048]{1,0:T(8,128)(2,1)S(1)} %pad_maximum_fusion.router_ref, ...), custom_call_target="tpu_custom_call" | custom-call | tf_op jit(solution)/shard_map/channel/pallas_call | solution.py:140
  84.2 0.0 copy-start.4
  84.3 0.8 copy-done.4
  85.0 0.8 copy-done.8
  85.8 2.9 %all-to-all-start.4 = ((bf16[32,4,2048]{2,1,0:T(4,128)(2,1)}), bf16[32,4,2048]{2,1,0:T(4,128)(2,1)S(1)}, u32[]{:S(2)}, u32[]{:S(2)}) async-start(bf16[32,4,2048]{2,1,0:T(4,128)(2,1)} %copy-done.4), calls=%async_computation.4 | async-start | bytes 1048576 | tf_op jit(solution)/shard_map/all_to_all | solution.py:235
  88.7 15.6 %all-to-all-done.4 = bf16[32,4,2048]{2,1,0:T(4,128)(2,1)S(1)} async-done(((bf16[32,4,2048]{2,1,0:T(4,128)(2,1)}), bf16[32,4,2048]{2,1,0:T(4,128)(2,1)S(1)}, u32[]{:S(2)}, u32[]{:S(2)}) %all-to-all-start.4) | async-done | bytes 524320 | tf_op jit(solution)/shard_map/all_to_all | solution.py:235
  104.3 0.2 convert_reduce_fusion
  104.6 0.9 fusion.14
  105.5 1.0 multiply_reduce_fusion
  106.4 1.5 %add_convert_fusion = bf16[4,2048]{1,0:T(4,128)(2,1)} fusion(f32[2048]{0:T(1024)} %param.42, f32[2048]{0:T(1024)} %param.41, f32[4]{0:T(128)S(1)} %add_rsqrt_fusion.1, f32[4]{0:T(128)S(1)} %broadcast_multiply_fusion.1, f32[4,2048]{1,0:T(4,128)S(1)} %convert_reduce_fusion, bf16[128,2048]{1,0:T(8,128)(2,1)} %copy-done.8, s32[]{:T(128)S(6)} %select_n.9), kind=kLoop, calls=%fused_computation.18 | loop fusion | flops 65536 | bytes 81956 | tf_op jit(solution)/shard_map/convert_element_type | solution.py:243
  (15 shorter events, 0.1 us)
Async XLA Ops:
  0.6 53.2 %copy-start = (bf16[1024,64]{0,1:T(8,128)(2,1)S(1)}, bf16[1024,64]{0,1:T(8,128)(2,1)}, u32[]{:S(2)}) copy-start(bf16[1024,64]{0,1:T(8,128)(2,1)} %param.30) | copy-start | bytes 393220
  0.6 23.9 %copy-start.15 = (bf16[2048,32]{0,1:T(8,128)(2,1)S(1)}, bf16[2048,32]{0,1:T(8,128)(2,1)}, u32[]{:S(2)}) copy-start(bf16[2048,32]{0,1:T(8,128)(2,1)} %param.27) | copy-start | bytes 393220
  0.7 23.9 %copy-start.16 = (bf16[2048,32]{0,1:T(8,128)(2,1)S(1)}, bf16[2048,32]{0,1:T(8,128)(2,1)}, u32[]{:S(2)}) copy-start(bf16[2048,32]{0,1:T(8,128)(2,1)} %param.26) | copy-start | bytes 393220
  1.7 27.9 %copy-start.11 = (f32[1024]{0:T(1024)S(1)}, f32[1024]{0:T(1024)}, u32[]{:S(2)}) copy-start(f32[1024]{0:T(1024)} %param.28) | copy-start | bytes 12292
  24.4 12.9 %copy-start.10 = (f32[4,8,128,128]{3,2,1,0:T(8,128)S(1)}, f32[4,8,128,128]{3,2,1,0:T(8,128)}, u32[]{:S(2)}) copy-start(f32[4,8,128,128]{3,2,1,0:T(8,128)} %param.23) | copy-start | bytes 6291460
  26.6 10.2 %all-to-all-start.1 = ((bf16[32,4,128]{2,1,0:T(4,128)(2,1)}), bf16[32,4,128]{2,1,0:T(4,128)(2,1)S(1)}, u32[]{:S(2)}, u32[]{:S(2)}) async-start(bf16[32,4,128]{2,1,0:T(4,128)(2,1)} %bitcast.3), calls=%async_computation.1 | async-start | bytes 65536 | tf_op jit(solution)/shard_map/all_to_all | solution.py:196
  38.6 1.3 %copy-start.9 = (f32[4,8,128,128]{3,2,1,0:T(8,128)}, f32[4,8,128,128]{3,2,1,0:T(8,128)S(1)}, u32[]{:S(2)}) copy-start(f32[4,8,128,128]{3,2,1,0:T(8,128)S(1)} %multiply_add_fusion) | copy-start | bytes 6291460
  39.9 1.2 %copy-start.14 = (f32[128]{0:T(128)S(1)}, f32[128]{0:T(128)}, u32[]{:S(2)}) copy-start(f32[128]{0:T(128)} %param.29) | copy-start | bytes 1540
  41.0 16.6 %copy-start.13 = (s32[128,2]{0,1:T(2,128)S(1)}, s32[128,2]{0,1:T(2,128)}, u32[]{:S(2)}) copy-start(s32[128,2]{0,1:T(2,128)} %param.43) | copy-start | bytes 3076
  41.0 16.6 %copy-start.12 = (bf16[2048]{0:T(1024)(128)(2,1)S(1)}, bf16[2048]{0:T(1024)(128)(2,1)}, u32[]{:S(2)}) copy-start(bf16[2048]{0:T(1024)(128)(2,1)} %param.34) | copy-start | bytes 12292
  41.0 32.2 %copy-start.1 = (bf16[2048,176]{0,1:T(8,128)(2,1)S(1)}, bf16[2048,176]{0,1:T(8,128)(2,1)}, u32[]{:S(2)}) copy-start(bf16[2048,176]{0,1:T(8,128)(2,1)} %param.35) | copy-start | bytes 2162692
  41.0 32.2 %copy-start.2 = (bf16[2048,176]{0,1:T(8,128)(2,1)S(1)}, bf16[2048,176]{0,1:T(8,128)(2,1)}, u32[]{:S(2)}) copy-start(bf16[2048,176]{0,1:T(8,128)(2,1)} %param.36) | copy-start | bytes 2162692
  41.0 32.2 %copy-start.3 = (bf16[176,2048]{1,0:T(8,128)(2,1)S(1)}, bf16[176,2048]{1,0:T(8,128)(2,1)}, u32[]{:S(2)}) copy-start(bf16[176,2048]{1,0:T(8,128)(2,1)} %dense_down_hbm.1) | copy-start | bytes 2162692
  41.0 32.2 %copy-start.6 = (f32[2048]{0:T(1024)S(1)}, f32[2048]{0:T(1024)}, u32[]{:S(2)}) copy-start(f32[2048]{0:T(1024)} %param.31) | copy-start | bytes 24580
  41.0 32.2 %copy-start.7 = (f32[2048]{0:T(1024)S(1)}, f32[2048]{0:T(1024)}, u32[]{:S(2)}) copy-start(f32[2048]{0:T(1024)} %param.32) | copy-start | bytes 24580
  54.9 18.2 %all-to-all-start.3 = ((bf16[32,64,128]{2,1,0:T(8,128)(2,1)}), bf16[32,64,128]{2,1,0:T(8,128)(2,1)S(1)}, u32[]{:S(2)}, u32[]{:S(2)}) async-start(bf16[32,64,128]{2,1,0:T(8,128)(2,1)} %broadcast_in_dim.16), calls=%async_computation.3 | async-start | bytes 1048576 | tf_op jit(solution)/shard_map/all_to_all | solution.py:41
  73.2 0.8 copy-start.5
  84.2 0.8 copy-start.4
  85.0 0.8 copy-start.8
  85.8 18.5 %all-to-all-start.4 = ((bf16[32,4,2048]{2,1,0:T(4,128)(2,1)}), bf16[32,4,2048]{2,1,0:T(4,128)(2,1)S(1)}, u32[]{:S(2)}, u32[]{:S(2)}) async-start(bf16[32,4,2048]{2,1,0:T(4,128)(2,1)} %copy-done.4), calls=%async_computation.4 | async-start | bytes 1048576 | tf_op jit(solution)/shard_map/all_to_all | solution.py:235
